TPU v7x, 512 devices: a whole 4x4x16 slice. The times are simulated.
512 devices in a mesh: fs: 64 (over z, y), tp: 8 (over x, core).
Axes of the slice: x: 4, y: 4, z: 16, core: 2. Of those that a mesh axis runs over, the one named last changes fastest.
Arguments:
- inputs: bfloat16 [16384, 2048], P('fs'), may hold values from -6 to 6
- query_cot: bfloat16 [16384, 1024], P('fs', 'tp'), may hold values from -0.046875 to 0.046875
- query_basis: bfloat16 [2048, 256], P('fs'), may hold values from -0.125 to 0.125
- query_master: float32 [2048, 1024], P('fs', 'tp'), may hold values from -3 to 3
- query_first: float32 [256, 1024], P('fs', 'tp'), may hold values from -4 to 4
- query_second: float32 [256, 1024], P('fs', 'tp'), may hold values from 0.02 to 4
Outputs:
- query_step: float32 [2048, 1024], P('fs', 'tp')
- query_first_new: float32 [256, 1024], P('fs', 'tp')
- query_second_new: float32 [256, 1024], P('fs', 'tp')
- query_copy: bfloat16 [2048, 1024], P('fs', 'tp')
All inputs are finite; a program needn't handle non-finite values.
Results may differ from a plain program's by a relative error of at most 0.0011.
Values may be sent and summed in bfloat16 or wider, within the bound.
No kernel may reach another device: no remote copies, remote signals or barrier semaphores. Data moves between devices by JAX's collectives and lax.ppermute only.
A program may use at most 64 MiB of HBM per device.

v0:
```python
import jax
import jax.numpy as jnp
from jax import lax
from jax.sharding import Mesh
from jax.sharding import PartitionSpec as P

HEADS = 8
DQK = 128
RANK = 256
TP = ("tp_0", "tp_1")
FS = ("fs_0", "fs_1")
FS_TP = ("fs_0", "fs_1", "tp_0", "tp_1")


CONTRACT = (((0,), (0,)), ((), ()))


def in_blocks(shard, dim, devices):
    before, after = (shard.shape[:dim], shard.shape[dim + 1 :])
    return jnp.moveaxis(shard.reshape(*before, devices, -1, *after), dim, 0)


def summed_on_arrival(shard, axis, dim):
    devices = lax.axis_size(axis)
    parts = lax.all_to_all(in_blocks(shard, dim, devices), axis, 0, 0, tiled=True)
    return jnp.sum(parts, axis=0)


def one_axis_at_a_time(shard, axes):
    for axis in axes:
        shard = lax.psum(shard, axis)
    return shard


def in_order(parts, dim):
    lengths = list(parts.shape[1:])
    lengths[dim] *= parts.shape[0]
    return jnp.moveaxis(parts, 0, dim).reshape(lengths)


def copy_for_each(shard, axis):
    copies = jnp.broadcast_to(shard, (lax.axis_size(axis), *shard.shape))
    return lax.all_to_all(copies, axis, split_axis=0, concat_axis=0, tiled=True)


def collect(shard, axis, dim):
    return in_order(copy_for_each(shard, axis), dim)


def moments(first, second, low_grad):
    first_new = 0.8 * first + 0.2 * low_grad
    second_new = 0.9 * second + 0.1 * low_grad * low_grad
    return (first_new, second_new, first_new / jnp.sqrt(second_new))


def head_sums(update, width):
    heads_local = update.shape[1] // width
    squares = jnp.sum((update * update).reshape(-1, heads_local, width), axis=(0, 2))
    offset = lax.axis_index(TP) * heads_local
    return lax.dynamic_update_slice(jnp.zeros((HEADS,), jnp.float32), squares, (offset,))


def apply_scale(update, totals, width):
    heads_local = update.shape[1] // width
    offset = lax.axis_index(TP) * heads_local
    head_mean = lax.dynamic_slice(totals, (offset,), (heads_local,)) / (RANK * width)
    whole_mean = jnp.sum(totals) / (RANK * HEADS * width)
    factor = 1.0 / jnp.sqrt(head_mean + whole_mean)
    return (update.reshape(-1, heads_local, width) * factor[None, :, None]).reshape(update.shape)


def body(inputs, query_cot, query_basis, query_master, query_first, query_second):
    basis_q = query_basis.astype(jnp.float32)
    gradient = summed_on_arrival(
        lax.dot_general(inputs, query_cot, CONTRACT, preferred_element_type=jnp.float32), FS, 0
    )
    low_parts = summed_on_arrival(
        lax.dot_general(basis_q, gradient, CONTRACT, precision=lax.Precision.HIGHEST), FS, 0
    )
    first_q, second_q, update_q = moments(query_first, query_second, low_parts)
    totals_q = one_axis_at_a_time(head_sums(update_q, DQK), FS_TP)
    scaled_q = apply_scale(update_q, totals_q, DQK)
    gathered_q = collect(scaled_q, FS, 0)
    step_q = jnp.dot(basis_q, gathered_q, precision=lax.Precision.HIGHEST)
    copy_q = (query_master + step_q).astype(jnp.bfloat16)
    return (step_q, first_q, second_q, copy_q)


def solution(mesh):
    torus = Mesh(mesh.devices.reshape(16, 4, 4, 2), ("fs_0", "fs_1", "tp_0", "tp_1"))
    in_specs = (P(FS, None), P(FS, TP), P(FS, None), P(FS, TP), P(FS, TP), P(FS, TP))
    out_specs = (P(FS, TP), P(FS, TP), P(FS, TP), P(FS, TP))
    return jax.shard_map(body, mesh=torus, in_specs=in_specs, out_specs=out_specs, check_vma=False)
```

profile of v0, /device:TPU:1, one launch (start us, length us, event | category | flops | bytes accessed | tf_op | source)
XLA Modules:
  0.0 177.7 jit_solution(7039905519884814700)
XLA Ops:
  0.6 0.0 copy-start
  0.6 1.2 copy-done
  1.9 1.3 fusion.2
  3.2 70.7 %all_to_all.15 = f32[64,32,128]{2,1,0:T(8,128)S(1)} all-to-all(f32[64,32,128]{2,1,0:T(8,128)S(1)} %bitcast.16), channel_id=1, replica_groups=mesh['fs_0'=16,'fs_1'=4,'tp_0'=4,'tp_1'=2] {'fs_0','fs_1'}, dimensions={0} | all-to-all | bytes 2097152 | tf_op jit(solution)/shard_map/all_to_all | solution.py:25
  73.9 0.1 reduce_sum.38
  74.0 0.6 copy-done.1
  74.6 0.3 convolution_bitcast_fusion
  74.9 0.7 copy.10
  75.6 8.6 %all-to-all-start.1 = ((f32[64,4,128]{2,1,0:T(4,128)}), f32[64,4,128]{2,1,0:T(4,128)S(1)}, u32[]{:S(2)}, u32[]{:S(2)}) async-start(f32[64,4,128]{2,1,0:T(4,128)} %bitcast.2), calls=%async_computation.1 | async-start | bytes 262144 | tf_op jit(solution)/shard_map/all_to_all | solution.py:25
  84.2 0.0 copy-start.5
  84.2 0.0 copy-start.6
  84.2 15.0 %all-to-all-done.1 = f32[64,4,128]{2,1,0:T(4,128)S(1)} async-done(((f32[64,4,128]{2,1,0:T(4,128)}), f32[64,4,128]{2,1,0:T(4,128)S(1)}, u32[]{:S(2)}, u32[]{:S(2)}) %all-to-all-start.1) | async-done | bytes 131104 | tf_op jit(solution)/shard_map/all_to_all | solution.py:25
  99.2 0.1 reduce_sum.39
  99.3 0.6 multiply_reduce_fusion
  99.9 0.8 dynamic_update_slice.3
  100.7 20.5 %psum.28 = f32[8]{0:T(128)S(1)} all-reduce(f32[8]{0:T(128)S(1)} %dynamic_update_slice.3), channel_id=1, replica_groups=mesh['fs_0'=16,'fs_1'=4,'tp_0'=4,'tp_1'=2] {'fs_0'}, use_global_device_ids=true, to_apply=%region_3.0 | all-reduce | flops 8 | bytes 64 | tf_op jit(solution)/shard_map/psum | solution.py:31
  121.2 7.4 %psum.29 = f32[8]{0:T(128)S(1)} all-reduce(f32[8]{0:T(128)S(1)} %psum.28), channel_id=1, replica_groups=mesh['fs_0'=16,'fs_1'=4,'tp_0'=4,'tp_1'=2] {'fs_1'}, use_global_device_ids=true, to_apply=%region_4.0 | all-reduce | flops 8 | bytes 64 | tf_op jit(solution)/shard_map/psum | solution.py:31
  128.6 8.5 %psum.30 = f32[8]{0:T(128)S(1)} all-reduce(f32[8]{0:T(128)S(1)} %psum.29), channel_id=1, replica_groups=mesh['fs_0'=16,'fs_1'=4,'tp_0'=4,'tp_1'=2] {'tp_0'}, use_global_device_ids=true, to_apply=%region_5.0 | all-reduce | flops 8 | bytes 64 | tf_op jit(solution)/shard_map/psum | solution.py:31
  137.1 16.3 %psum.31 = f32[8]{0:T(128)S(1)} all-reduce(f32[8]{0:T(128)S(1)} %psum.30), channel_id=1, replica_groups=mesh['fs_0'=16,'fs_1'=4,'tp_0'=4,'tp_1'=2] {'tp_1'}, use_global_device_ids=true, to_apply=%region_6.0 | all-reduce | flops 8 | bytes 64 | tf_op jit(solution)/shard_map/psum | solution.py:31
  153.4 0.6 dynamic_slice.3
  154.0 0.6 reduce_sum.42
  156.0 0.0 copy-start.2
  156.0 20.9 %all_to_all.16 = f32[64,4,128]{2,1,0:T(4,128)S(1)} all-to-all(f32[64,4,128]{2,1,0:T(4,128)S(1)} %broadcast_in_dim.4), channel_id=1, replica_groups=mesh['fs_0'=16,'fs_1'=4,'tp_0'=4,'tp_1'=2] {'fs_0','fs_1'}, dimensions={0} | all-to-all | bytes 262144 | tf_op jit(solution)/shard_map/all_to_all | solution.py:43
  176.9 0.8 add_convert_fusion
  (11 shorter events, 0.0 us)
Async XLA Ops:
  0.6 1.2 copy-start
  73.9 0.7 copy-start.1
  75.6 23.6 %all-to-all-start.1 = ((f32[64,4,128]{2,1,0:T(4,128)}), f32[64,4,128]{2,1,0:T(4,128)S(1)}, u32[]{:S(2)}, u32[]{:S(2)}) async-start(f32[64,4,128]{2,1,0:T(4,128)} %bitcast.2), calls=%async_computation.1 | async-start | bytes 262144 | tf_op jit(solution)/shard_map/all_to_all | solution.py:25
  84.2 15.1 %copy-start.5 = (f32[4,128]{1,0:T(4,128)S(1)}, f32[4,128]{1,0:T(4,128)}, u32[]{:S(2)}) copy-start(f32[4,128]{1,0:T(4,128)} %param.11) | copy-start | bytes 6148
  84.2 15.1 %copy-start.6 = (f32[4,128]{1,0:T(4,128)S(1)}, f32[4,128]{1,0:T(4,128)}, u32[]{:S(2)}) copy-start(f32[4,128]{1,0:T(4,128)} %param.10) | copy-start | bytes 6148
  99.9 56.0 %copy-start.3 = (f32[4,128]{1,0:T(4,128)}, f32[4,128]{1,0:T(4,128)S(1)}, u32[]{:S(2)}) copy-start(f32[4,128]{1,0:T(4,128)S(1)} %get-tuple-element.5) | copy-start | bytes 6148
  99.9 56.0 %copy-start.4 = (f32[4,128]{1,0:T(4,128)}, f32[4,128]{1,0:T(4,128)S(1)}, u32[]{:S(2)}) copy-start(f32[4,128]{1,0:T(4,128)S(1)} %get-tuple-element.6) | copy-start | bytes 6148
  156.0 20.9 %copy-start.2 = (f32[32,128]{1,0:T(8,128)S(1)}, f32[32,128]{1,0:T(8,128)}, u32[]{:S(2)}) copy-start(f32[32,128]{1,0:T(8,128)} %param.9) | copy-start | bytes 49156
where the time goes:
time: 179 us; the launch traced here: 178 us
  blocking collectives  144 us (80%)
  waiting for transfers between devices  15 us (8%)
  starting transfers between devices  8.58 us (5%)
  local copies, waits for them, and re-layouts  3.97 us (2%)
  matrix products  2.37 us (1%)
  between operations  2.07 us (1%)
    all_to_all x1, blocking collectives, summed_on_arrival(): lax.all_to_all(in_blocks(shard, dim, devices), axis, 0, 0, tiled=True)  70.7 us
    psum x4, blocking collectives, one_axis_at_a_time(): shard = lax.psum(shard, axis)  52.7 us
    all_to_all x1, blocking collectives, copy_for_each(): return lax.all_to_all(copies, axis, split_axis=0, concat_axis=0, tiled=True)  20.9 us
    all_to_all x1, waiting for transfers between devices, summed_on_arrival(): lax.all_to_all(in_blocks(shard, dim, devices), axis, 0, 0, tiled=True)  15 us
    all_to_all x1, starting transfers between devices, summed_on_arrival(): lax.all_to_all(in_blocks(shard, dim, devices), axis, 0, 0, tiled=True)  8.58 us
  transfers between devices with their start and end apart: 1, of which 1 were waited for; matrix products, arithmetic and copies ran while one was open for 0% of the time, Pallas kernels for 0%

commit v1 on v0

v1 whole, which is shorter than its diff:
```python
import jax
import jax.numpy as jnp
from jax import lax
from jax.experimental import pallas as pl
from jax.experimental.pallas import tpu as pltpu
from jax.sharding import Mesh
from jax.sharding import PartitionSpec as P

HEADS = 8
DQK = 128
RANK = 256
NZ, NY, NX, NC = 16, 4, 4, 2
TP = ("x", "c")
FS = ("z", "y")
PLANE = ("y", "x", "c")
PER = RANK // HEADS
KEPT = 24

F32 = jnp.float32
BF16 = jnp.bfloat16


def vmem(count):
    return [pl.BlockSpec(memory_space=pltpu.VMEM)] * count


def call(kernel, out, operands, scalars=(), scratch=(), flops=200_000, limit=4 << 20):
    single = not isinstance(out, (list, tuple))
    moved = sum(a.size * a.dtype.itemsize for a in operands)
    return pl.pallas_call(
        kernel,
        out_shape=out,
        in_specs=[pl.BlockSpec(memory_space=pltpu.SMEM)] * len(scalars) + vmem(len(operands)),
        out_specs=vmem(1)[0] if single else vmem(len(out)),
        scratch_shapes=list(scratch),
        cost_estimate=pl.CostEstimate(flops=flops, bytes_accessed=moved, transcendentals=0),
        compiler_params=pltpu.CompilerParams(vmem_limit_bytes=limit),
    )(*scalars, *operands)


def exchange(parts, axes):
    return lax.all_to_all(parts, axes, 0, 0, tiled=True)


def pick_kernel(place, basis, out):
    j = place[0]
    rank = lax.broadcasted_iota(jnp.int32, (RANK, PER), 0)
    slot = lax.broadcasted_iota(jnp.int32, (RANK, PER), 1)
    wanted = (slot // 2) * (RANK // NZ) + 2 * j + slot % 2
    chosen = (rank == wanted).astype(F32).astype(BF16)
    mine = jnp.dot(basis[...], chosen, preferred_element_type=F32)
    wide = jnp.concatenate([mine[8 * q : 8 * q + 8] for q in range(4)], axis=1)
    out[...] = jnp.broadcast_to(wide.astype(BF16)[None], out.shape)


def project_kernel(place, inputs, columns, own, other, out):
    x, c = place[1], place[2]
    got = columns[...].astype(F32)
    basis = jnp.concatenate([got[:, :, PER * q : PER * q + PER] for q in range(4)], axis=1)
    basis = basis.reshape(inputs.shape[1], PER).astype(BF16)
    low = jnp.dot(inputs[...], basis, preferred_element_type=F32)
    high = low.astype(BF16)
    rest = (low - high.astype(F32)).astype(BF16)
    both = jnp.concatenate([high.astype(F32).T, rest.astype(F32).T], axis=0).astype(BF16)
    for cots, core in ((own, c), (other, 1 - c)):
        for s in range(NX):
            part = jnp.dot(both, cots[s], preferred_element_type=F32)
            part = part[:PER] + part[PER:]
            row = 4 * lax.rem(x + NX - s, NX) + 2 * core
            for z in range(NZ):
                out[z, pl.ds(row, 2), :] = part[2 * z : 2 * z + 2]


def sum_kernel(parts, first, second, out):
    shape = (NY * HEADS, 2 * HEADS, DQK)
    out[:, : 2 * HEADS, :] = jnp.broadcast_to(jnp.sum(parts[...], axis=0)[None], shape)
    pair = jnp.concatenate([first[...], second[...]], axis=0)
    out[:, 2 * HEADS :, :] = jnp.broadcast_to(pair[None], (NY * HEADS, 8, DQK))


def moments_kernel(place, parts, out, first_own, second_own, fn, sn, un):
    j, y = place[0], place[3]
    low = jnp.sum(parts[:, : 2 * HEADS, :].reshape(NY, HEADS, 2 * HEADS, DQK), axis=0)

    def moment(start):
        rows = []
        for i in range(2):
            at = start + 2 * i
            one = [
                jnp.concatenate([parts[b * HEADS + h, at : at + 2, :] for h in range(HEADS)], axis=0)
                for b in range(NY)
            ]
            rows.append(jnp.stack(one))
        return jnp.stack(rows, axis=1).reshape(HEADS, 2 * HEADS, DQK)

    first_new = 0.8 * moment(2 * HEADS) + 0.2 * low
    second_new = 0.9 * moment(2 * HEADS + 4) + 0.1 * low * low
    update = first_new / jnp.sqrt(second_new)
    fn[...] = first_new
    sn[...] = second_new
    un[...] = update
    rows = pl.ds(2 * j, 2)
    for i in range(2):
        first_own[2 * i : 2 * i + 2, :] = fn[2 * y + i, rows, :]
        second_own[2 * i : 2 * i + 2, :] = sn[2 * y + i, rows, :]
    total = jnp.sum(jnp.sum(update * update, axis=(0, 1), keepdims=True), axis=2, keepdims=True)
    own = jnp.concatenate([un[i, rows, :] for i in range(HEADS)], axis=0)
    out[:, : 2 * HEADS, :] = jnp.broadcast_to(own[None], (NZ, 2 * HEADS, DQK))
    out[:, 2 * HEADS :, :] = jnp.broadcast_to(total, (NZ, 8, DQK))


def step_kernel(parts, basis, master, step_out, copy_out):
    update = parts[:, : 2 * HEADS, :].reshape(RANK, DQK)
    whole = jnp.sum(parts[:, 2 * HEADS, :], axis=0, keepdims=True) / (RANK * HEADS * DQK)
    squares = jnp.sum(update * update, axis=0, keepdims=True)
    head = jnp.sum(squares, axis=1, keepdims=True) / (RANK * DQK)
    factor = 1.0 / jnp.sqrt(head + whole)
    high = update.astype(BF16)
    left = update - high.astype(F32)
    mid = left.astype(BF16)
    small = (left - mid.astype(F32)).astype(BF16)
    rows = basis[...]
    step = jnp.dot(rows, small, preferred_element_type=F32)
    step += jnp.dot(rows, mid, preferred_element_type=F32)
    step += jnp.dot(rows, high, preferred_element_type=F32)
    step *= factor
    step_out[...] = step
    copy_out[...] = (master[...] + step).astype(BF16)


def rotated(shard, axis, by):
    size = lax.axis_size(axis)
    return lax.ppermute(shard, axis, [(i, (i + by) % size) for i in range(size)])


def whole(inputs, query_cot, query_basis, query_master, query_first, query_second):
    sds = jax.ShapeDtypeStruct
    at = [lax.axis_index(axis) for axis in (TP, "x", "c", "y")]
    place = jnp.stack(at).astype(jnp.int32)
    picked = call(pick_kernel, sds((NZ * NY, 8, DQK), BF16), (query_basis,), (place,))
    columns = exchange(picked, FS)
    own = jnp.stack([query_cot] + [rotated(query_cot, "x", s) for s in range(1, NX)])
    other = rotated(own, "c", 1)
    low = call(
        project_kernel,
        sds((NZ, 2 * HEADS, DQK), F32),
        (inputs, columns, own, other),
        (place,),
        flops=400_000_000,
        limit=16 << 20,
    )
    low = exchange(low, "z")
    low = call(sum_kernel, sds((NY * HEADS, KEPT, DQK), F32), (low, query_first, query_second))
    low = exchange(low, PLANE)
    small = sds(query_first.shape, F32)
    update, first_new, second_new = call(
        moments_kernel,
        (sds((NZ, KEPT, DQK), F32), small, small),
        (low,),
        (place,),
        scratch=[pltpu.VMEM((HEADS, 2 * HEADS, DQK), F32)] * 3,
    )
    update = exchange(update, "z")
    step, copy = call(
        step_kernel,
        (sds(query_master.shape, F32), sds(query_master.shape, BF16)),
        (update, query_basis, query_master),
    )
    return (step, first_new, second_new, copy)


def solution(mesh):
    torus = Mesh(mesh.devices.reshape(NZ, NY, NX, NC), ("z", "y", "x", "c"))
    in_specs = (P(FS, None), P(FS, TP), P(FS, None), P(FS, TP), P(FS, TP), P(FS, TP))
    out_specs = (P(FS, TP), P(FS, TP), P(FS, TP), P(FS, TP))
    return jax.shard_map(whole, mesh=torus, in_specs=in_specs, out_specs=out_specs, check_vma=False)
```

time: 179 us -> 108 us (0.60)
  the two profiles are of different devices: /device:TPU:1 before, /device:TPU:32 now
where the time goes in v1:
time: 108 us; the launch traced here: 107 us
  blocking collectives  62.9 us (58%)
  starting transfers between devices  31.2 us (29%)
  waiting for transfers between devices  5.42 us (5%)
  Pallas kernels  4.71 us (4%)
  local copies, waits for them, and re-layouts  1.87 us (2%)
    all_to_all x3, blocking collectives, exchange(): return lax.all_to_all(parts, axes, 0, 0, tiled=True)  62.9 us
    all_to_all x1, starting transfers between devices, exchange(): return lax.all_to_all(parts, axes, 0, 0, tiled=True)  18.5 us
    ppermute x4, starting transfers between devices, rotated(): lax.ppermute(shard, axis, [(i, (i + by) % size) for i in range(size)])  12.7 us
    ppermute x4, waiting for transfers between devices, rotated(): lax.ppermute(shard, axis, [(i, (i + by) % size) for i in range(size)])  5.42 us
    pallas_call x5, Pallas kernels, call(): pl.pallas_call(kernel, out_shape=out, in_specs=[pl.BlockSpec(memory_space...  4.71 us
  transfers between devices with their start and end apart: 5, of which 2 were waited for; matrix products, arithmetic and copies ran while one was open for 0% of the time, Pallas kernels for 0%

profile of v1, /device:TPU:32, one launch (start us, length us, event | category | flops | bytes accessed | tf_op | source)
XLA Modules:
  0.0 107.0 jit_solution(14495200299379004208)
XLA Ops:
  0.6 0.0 copy-start.1
  0.6 0.1 pad_add_fusion.place
  0.7 0.6 copy-done.1
  1.3 1.4 %shard_map.93 = bf16[64,8,128]{2,1,0:T(8,128)(2,1)} custom-call(s32[4]{0:T(128)S(1)} %pad_add_fusion.place, bf16[32,256]{1,0:T(8,128)(2,1)S(1)} %copy-done.1), custom_call_target="tpu_custom_call" | custom-call | flops 200000 | bytes 16384 | tf_op jit(solution)/shard_map/pallas_call | solution.py:30
  2.8 18.5 %all-to-all-start = ((bf16[64,8,128]{2,1,0:T(8,128)(2,1)}), bf16[64,8,128]{2,1,0:T(8,128)(2,1)S(1)}, u32[]{:S(2)}, u32[]{:S(2)}) async-start(bf16[64,8,128]{2,1,0:T(8,128)(2,1)} %shard_map.93), calls=%async_computation | async-start | bytes 262144 | tf_op jit(solution)/shard_map/all_to_all | solution.py:42
  21.3 0.0 copy-done.5
  21.3 3.4 %collective-permute-start = (bf16[256,128]{1,0:T(8,128)(2,1)S(1)}, bf16[256,128]{1,0:T(8,128)(2,1)S(1)}, u32[]{:S(2)}, u32[]{:S(2)}) collective-permute-start(bf16[256,128]{1,0:T(8,128)(2,1)S(1)} %copy-done.5), channel_id=1, source_target_pairs={{0,2},{2,4},{4,6},{6,0},{1,3},{3,5},{5,7},{7,1},{8,10},{10,12},{12... | collective-permute-start | bytes 196616 | tf_op jit(solution)/shard_map/ppermute | solution.py:133
  24.7 3.7 %collective-permute-start.2 = (bf16[256,128]{1,0:T(8,128)(2,1)S(1)}, bf16[256,128]{1,0:T(8,128)(2,1)S(1)}, u32[]{:S(2)}, u32[]{:S(2)}) collective-permute-start(bf16[256,128]{1,0:T(8,128)(2,1)S(1)} %copy-done.5), channel_id=1, source_target_pairs={{0,6},{2,0},{4,2},{6,4},{1,7},{3,1},{5,3},{7,5},{8,14},{10,8},{12,... | collective-permute-start | bytes 196616 | tf_op jit(solution)/shard_map/ppermute | solution.py:133
  28.4 3.7 %collective-permute-start.1 = (bf16[256,128]{1,0:T(8,128)(2,1)S(1)}, bf16[256,128]{1,0:T(8,128)(2,1)S(1)}, u32[]{:S(2)}, u32[]{:S(2)}) collective-permute-start(bf16[256,128]{1,0:T(8,128)(2,1)S(1)} %copy-done.5), channel_id=1, source_target_pairs={{0,4},{2,6},{4,0},{6,2},{1,5},{3,7},{5,1},{7,3},{8,12},{10,14},{12... | collective-permute-start | bytes 196616 | tf_op jit(solution)/shard_map/ppermute | solution.py:133
  32.1 0.0 collective-permute-done
  32.1 0.0 collective-permute-done.2
  32.1 3.9 %collective-permute-done.1 = bf16[256,128]{1,0:T(8,128)(2,1)S(1)} collective-permute-done((bf16[256,128]{1,0:T(8,128)(2,1)S(1)}, bf16[256,128]{1,0:T(8,128)(2,1)S(1)}, u32[]{:S(2)}, u32[]{:S(2)}) %collective-permute-start.1) | collective-permute-done | bytes 65568 | tf_op jit(solution)/shard_map/ppermute | solution.py:133
  36.1 1.9 %collective-permute-start.3 = (bf16[4,256,128]{2,1,0:T(8,128)(2,1)S(1)}, bf16[4,256,128]{2,1,0:T(8,128)(2,1)S(1)}, u32[]{:S(2)}, u32[]{:S(2)}) collective-permute-start(bf16[4,256,128]{2,1,0:T(8,128)(2,1)S(1)} %pad_maximum_fusion.own), channel_id=1, source_target_pairs={{0,1},{1,0},{2,3},{3,2},{4,5},{5,4},{6,7},{7,6},{8,9},{9,8},{10,11... | collective-permute-start | bytes 786440 | tf_op jit(solution)/shard_map/ppermute | solution.py:133
  38.0 1.5 %collective-permute-done.3.other = bf16[4,256,128]{2,1,0:T(8,128)(2,1)S(1)} collective-permute-done((bf16[4,256,128]{2,1,0:T(8,128)(2,1)S(1)}, bf16[4,256,128]{2,1,0:T(8,128)(2,1)S(1)}, u32[]{:S(2)}, u32[]{:S(2)}) %collective-permute-start.3) | collective-permute-done | bytes 262176 | tf_op jit(solution)/shard_map/ppermute | solution.py:133
  39.5 0.0 all-to-all-done.columns
  39.5 1.2 %copy-done = bf16[256,2048]{1,0:T(8,128)(2,1)S(1)} copy-done((bf16[256,2048]{1,0:T(8,128)(2,1)S(1)}, bf16[256,2048]{1,0:T(8,128)(2,1)}, u32[]{:S(2)}) %copy-start) | copy-done | bytes 1048600
  40.7 1.3 %shard_map.94 = f32[16,16,128]{2,1,0:T(8,128)S(1)} custom-call(s32[4]{0:T(128)S(1)} %pad_add_fusion.place, bf16[256,2048]{1,0:T(8,128)(2,1)S(1)} %copy-done, bf16[64,8,128]{2,1,0:T(8,128)(2,1)S(1)} %all-to-all-done.columns, bf16[4,256,128]{2,1,0:T(8,128)(2,1)S(1)} %pad_maximum_fusion.own, bf16[4,256,128]{2,1,0:T(8,128)(2,1)S(1)} %collective-permute-done.3.other), custom_call_target="tpu_custom_call" | custom-call | flops 400000000 | bytes 1703936 | tf_op jit(solution)/shard_map/pallas_call | solution.py:30
  42.0 0.0 copy-start.3
  42.0 0.0 copy-start.4
  42.1 25.9 %all_to_all.20.parts = f32[16,16,128]{2,1,0:T(8,128)S(1)} all-to-all(f32[16,16,128]{2,1,0:T(8,128)S(1)} %shard_map.94), channel_id=1, replica_groups=mesh['z'=16,'y'=4,'x'=4,'c'=2] {'z'}, dimensions={0} | all-to-all | bytes 262144 | tf_op jit(solution)/shard_map/all_to_all | solution.py:42
  68.0 15.9 %all_to_all.21.parts = f32[32,24,128]{2,1,0:T(8,128)S(1)} all-to-all(f32[32,24,128]{2,1,0:T(8,128)S(1)} %shard_map.95), channel_id=1, replica_groups=mesh['z'=16,'y'=4,'x'=4,'c'=2] {'y','x','c'}, dimensions={0} | all-to-all | bytes 786432 | tf_op jit(solution)/shard_map/all_to_all | solution.py:42
  83.9 1.2 %shard_map.96 = (f32[16,24,128]{2,1,0:T(8,128)S(1)}, f32[4,128]{1,0:T(4,128)}, f32[4,128]{1,0:T(4,128)}) custom-call(s32[4]{0:T(128)S(1)} %pad_add_fusion.place, f32[32,24,128]{2,1,0:T(8,128)S(1)} %all_to_all.21.parts), custom_call_target="tpu_custom_call" | custom-call | flops 200000 | bytes 393216 | tf_op jit(solution)/shard_map/pallas_call | solution.py:30
  85.0 21.1 %all_to_all.22.parts = f32[16,24,128]{2,1,0:T(8,128)S(1)} all-to-all(f32[16,24,128]{2,1,0:T(8,128)S(1)} %get-tuple-element.9), channel_id=1, replica_groups=mesh['z'=16,'y'=4,'x'=4,'c'=2] {'z'}, dimensions={0} | all-to-all | bytes 393216 | tf_op jit(solution)/shard_map/all_to_all | solution.py:42
  106.2 0.8 shard_map.97
  (8 shorter events, 0.1 us)
Async XLA Ops:
  0.6 0.7 copy-start.1
  2.8 18.5 %copy-start.5 = (bf16[256,128]{1,0:T(8,128)(2,1)S(1)}, bf16[256,128]{1,0:T(8,128)(2,1)}, u32[]{:S(2)}) copy-start(bf16[256,128]{1,0:T(8,128)(2,1)} %param.7) | copy-start | bytes 196612
  2.8 36.7 %all-to-all-start = ((bf16[64,8,128]{2,1,0:T(8,128)(2,1)}), bf16[64,8,128]{2,1,0:T(8,128)(2,1)S(1)}, u32[]{:S(2)}, u32[]{:S(2)}) async-start(bf16[64,8,128]{2,1,0:T(8,128)(2,1)} %shard_map.93), calls=%async_computation | async-start | bytes 262144 | tf_op jit(solution)/shard_map/all_to_all | solution.py:42
  21.3 10.8 %collective-permute-start = (bf16[256,128]{1,0:T(8,128)(2,1)S(1)}, bf16[256,128]{1,0:T(8,128)(2,1)S(1)}, u32[]{:S(2)}, u32[]{:S(2)}) collective-permute-start(bf16[256,128]{1,0:T(8,128)(2,1)S(1)} %copy-done.5), channel_id=1, source_target_pairs={{0,2},{2,4},{4,6},{6,0},{1,3},{3,5},{5,7},{7,1},{8,10},{10,12},{12... | collective-permute-start | bytes 196616 | tf_op jit(solution)/shard_map/ppermute | solution.py:133
  24.7 7.4 %collective-permute-start.2 = (bf16[256,128]{1,0:T(8,128)(2,1)S(1)}, bf16[256,128]{1,0:T(8,128)(2,1)S(1)}, u32[]{:S(2)}, u32[]{:S(2)}) collective-permute-start(bf16[256,128]{1,0:T(8,128)(2,1)S(1)} %copy-done.5), channel_id=1, source_target_pairs={{0,6},{2,0},{4,2},{6,4},{1,7},{3,1},{5,3},{7,5},{8,14},{10,8},{12,... | collective-permute-start | bytes 196616 | tf_op jit(solution)/shard_map/ppermute | solution.py:133
  28.4 7.7 %collective-permute-start.1 = (bf16[256,128]{1,0:T(8,128)(2,1)S(1)}, bf16[256,128]{1,0:T(8,128)(2,1)S(1)}, u32[]{:S(2)}, u32[]{:S(2)}) collective-permute-start(bf16[256,128]{1,0:T(8,128)(2,1)S(1)} %copy-done.5), channel_id=1, source_target_pairs={{0,4},{2,6},{4,0},{6,2},{1,5},{3,7},{5,1},{7,3},{8,12},{10,14},{12... | collective-permute-start | bytes 196616 | tf_op jit(solution)/shard_map/ppermute | solution.py:133
  36.1 3.4 %collective-permute-start.3 = (bf16[4,256,128]{2,1,0:T(8,128)(2,1)S(1)}, bf16[4,256,128]{2,1,0:T(8,128)(2,1)S(1)}, u32[]{:S(2)}, u32[]{:S(2)}) collective-permute-start(bf16[4,256,128]{2,1,0:T(8,128)(2,1)S(1)} %pad_maximum_fusion.own), channel_id=1, source_target_pairs={{0,1},{1,0},{2,3},{3,2},{4,5},{5,4},{6,7},{7,6},{8,9},{9,8},{10,11... | collective-permute-start | bytes 786440 | tf_op jit(solution)/shard_map/ppermute | solution.py:133
  39.5 1.2 %copy-start = (bf16[256,2048]{1,0:T(8,128)(2,1)S(1)}, bf16[256,2048]{1,0:T(8,128)(2,1)}, u32[]{:S(2)}) copy-start(bf16[256,2048]{1,0:T(8,128)(2,1)} %inputs.1) | copy-start | bytes 3145732
  42.0 25.9 %copy-start.3 = (f32[4,128]{1,0:T(4,128)S(1)}, f32[4,128]{1,0:T(4,128)}, u32[]{:S(2)}) copy-start(f32[4,128]{1,0:T(4,128)} %first.1) | copy-start | bytes 6148
  42.0 25.9 %copy-start.4 = (f32[4,128]{1,0:T(4,128)S(1)}, f32[4,128]{1,0:T(4,128)}, u32[]{:S(2)}) copy-start(f32[4,128]{1,0:T(4,128)} %second.1) | copy-start | bytes 6148
  85.0 21.1 %copy-start.2 = (f32[32,128]{1,0:T(8,128)S(1)}, f32[32,128]{1,0:T(8,128)}, u32[]{:S(2)}) copy-start(f32[32,128]{1,0:T(8,128)} %master.1) | copy-start | bytes 49156

commit v2 on v1

v2 whole, which is shorter than its diff:
```python
import jax
import jax.numpy as jnp
from jax import lax
from jax.experimental import pallas as pl
from jax.experimental.pallas import tpu as pltpu
from jax.sharding import Mesh
from jax.sharding import PartitionSpec as P

HEADS = 8
DQK = 128
RANK = 256
ZH, ZL, NY, NX, NC = 8, 2, 4, 4, 2
TP = ("x", "c")
FS = ("zh", "zl", "y")
NEAR = ("zl", "y")
GROUPS = ZL * NY
PER = RANK // GROUPS
OWN = PER // ZH

F32 = jnp.float32
BF16 = jnp.bfloat16


def vmem(count):
    return [pl.BlockSpec(memory_space=pltpu.VMEM)] * count


def call(kernel, out, operands, scalars=(), scratch=(), specs=None, flops=200_000, limit=4 << 20, name=None):
    single = not isinstance(out, (list, tuple))
    moved = sum(a.size * a.dtype.itemsize for a in operands)
    return pl.pallas_call(
        kernel,
        out_shape=out,
        in_specs=[pl.BlockSpec(memory_space=pltpu.SMEM)] * len(scalars) + (specs or vmem(len(operands))),
        out_specs=vmem(1)[0] if single else vmem(len(out)),
        scratch_shapes=list(scratch),
        cost_estimate=pl.CostEstimate(flops=flops, bytes_accessed=moved, transcendentals=0),
        compiler_params=pltpu.CompilerParams(vmem_limit_bytes=limit),
        name=name,
    )(*scalars, *operands)


def exchange(parts, axes, name):
    with jax.named_scope(name):
        return lax.all_to_all(parts, axes, 0, 0, tiled=True)


def copies(block, count):
    return jnp.broadcast_to(block[None], (count, *block.shape))


def pick_kernel(place, inputs, basis, out, held, rows, sems):
    near = pltpu.make_async_copy(basis, rows, sems.at[0])
    far = pltpu.make_async_copy(inputs, held, sems.at[1])
    near.start()
    far.start()
    rank = lax.broadcasted_iota(jnp.int32, (RANK, PER), 0)
    slot = lax.broadcasted_iota(jnp.int32, (RANK, PER), 1)
    wanted = (slot // OWN) * PER + OWN * place[0] + slot % OWN
    chosen = (rank == wanted).astype(F32).astype(BF16)
    near.wait()
    mine = jnp.dot(rows[...], chosen, preferred_element_type=F32)
    wide = jnp.concatenate([mine[8 * q : 8 * q + 8] for q in range(4)], axis=1)
    out[...] = copies(wide.astype(BF16), out.shape[0])
    far.wait()


def project_kernel(inputs, columns, out):
    got = columns[...].astype(F32)
    basis = jnp.concatenate([got[:, :, PER * q : PER * q + PER] for q in range(4)], axis=1)
    basis = basis.reshape(inputs.shape[1], PER).astype(BF16)
    low = jnp.dot(inputs[...], basis, preferred_element_type=F32)
    high = low.astype(BF16)
    rest = (low - high.astype(F32)).astype(BF16)
    both = jnp.concatenate([high.astype(F32).T, rest.astype(F32).T], axis=0).astype(BF16)
    out[...] = copies(both, out.shape[0])


def low_kernel(both, cot, out):
    low = both[...].reshape(GROUPS * 2 * PER, both.shape[2])
    low = jnp.dot(low, cot[...], preferred_element_type=F32).reshape(GROUPS, 2 * PER, DQK)
    out[...] = low[:, :PER] + low[:, PER:]


def sum_kernel(parts, first, second, out):
    out[:, :PER, :] = copies(jnp.sum(parts[...], axis=0), ZH)
    pair = jnp.concatenate([first[...], second[...]], axis=0)
    out[:, PER:, :] = copies(pair, ZH)


def moments_kernel(place, parts, out, first_own, second_own, fn, sn):
    low = jnp.sum(parts[:, :PER, :], axis=0)
    first = jnp.concatenate([parts[z, PER : PER + OWN, :] for z in range(ZH)], axis=0)
    second = jnp.concatenate([parts[z, PER + OWN : PER + 2 * OWN, :] for z in range(ZH)], axis=0)
    first_new = 0.8 * first + 0.2 * low
    second_new = 0.9 * second + 0.1 * low * low
    fn[...] = first_new
    sn[...] = second_new
    out[...] = copies(first_new / jnp.sqrt(second_new), GROUPS)
    rows = pl.ds(OWN * place[1], OWN)
    first_own[...] = fn[rows, :]
    second_own[...] = sn[rows, :]


def apply_kernel(parts, basis, squares_out, step_out):
    update = jnp.concatenate(
        [parts[g, OWN * z : OWN * (z + 1), :] for z in range(ZH) for g in range(GROUPS)], axis=0
    )
    squares = jnp.sum(jnp.sum(update * update, axis=0, keepdims=True), axis=1, keepdims=True)
    squares_out[...] = jnp.broadcast_to(squares[None], squares_out.shape)
    high = update.astype(BF16)
    left = update - high.astype(F32)
    mid = left.astype(BF16)
    small = (left - mid.astype(F32)).astype(BF16)
    rows = basis[...]
    step = jnp.dot(rows, small, preferred_element_type=F32)
    step += jnp.dot(rows, mid, preferred_element_type=F32)
    step_out[...] = step + jnp.dot(rows, high, preferred_element_type=F32)


def scale_kernel(squares, own, raw, master, first, second, step_out, first_out, second_out, copy_out):
    whole = jnp.sum(squares[...], axis=0) / (RANK * HEADS * DQK)
    head = own[0] / (RANK * DQK)
    step = raw[...] * (1.0 / jnp.sqrt(head + whole))
    step_out[...] = step
    copy_out[...] = (master[...] + step).astype(BF16)
    first_out[...] = first[...]
    second_out[...] = second[...]


def body(inputs, query_cot, query_basis, query_master, query_first, query_second):
    sds = jax.ShapeDtypeStruct
    place = jnp.stack([lax.axis_index(TP), lax.axis_index("zh")]).astype(jnp.int32)
    tokens, small = inputs.shape[0], sds(query_first.shape, F32)
    columns, held = call(
        pick_kernel,
        (sds((ZH * GROUPS, 8, DQK), BF16), sds(inputs.shape, BF16)),
        (inputs, query_basis),
        (place,),
        specs=[pl.BlockSpec(memory_space=pltpu.HBM)] * 2,
        scratch=[pltpu.VMEM(query_basis.shape, BF16), pltpu.SemaphoreType.DMA((2,))],
        name="pick",
    )
    columns = exchange(columns, FS, "columns")
    both = call(
        project_kernel,
        sds((GROUPS, 2 * PER, tokens), BF16),
        (held, columns),
        flops=400_000_000,
        limit=16 << 20,
        name="project",
    )
    both = exchange(both, TP, "ranks")
    low = call(low_kernel, sds((GROUPS, PER, DQK), F32), (both, query_cot), name="low")
    low = exchange(low, NEAR, "near_sum")
    low = call(
        sum_kernel,
        sds((ZH, PER + 2 * OWN, DQK), F32),
        (low, query_first, query_second),
        name="sum_near",
    )
    low = exchange(low, "zh", "far_sum")
    update, first_new, second_new = call(
        moments_kernel,
        (sds((GROUPS, PER, DQK), F32), small, small),
        (low,),
        (place,),
        scratch=[pltpu.VMEM((PER, DQK), F32)] * 2,
        name="moments",
    )
    update = exchange(update, NEAR, "updates")
    squares, step = call(
        apply_kernel,
        (sds((HEADS, 1, DQK), F32), sds(query_master.shape, F32)),
        (update, query_basis),
        name="apply",
    )
    heads = exchange(squares, TP, "squares")
    step, first_new, second_new, copy = call(
        scale_kernel,
        (sds(query_master.shape, F32), small, small, sds(query_master.shape, BF16)),
        (heads, squares, step, query_master, first_new, second_new),
        name="scale",
    )
    return (step, first_new, second_new, copy)


def solution(mesh):
    torus = Mesh(mesh.devices.reshape(ZH, ZL, NY, NX, NC), (*FS, *TP))
    in_specs = (P(FS, None), P(FS, TP), P(FS, None), P(FS, TP), P(FS, TP), P(FS, TP))
    out_specs = (P(FS, TP), P(FS, TP), P(FS, TP), P(FS, TP))
    return jax.shard_map(body, mesh=torus, in_specs=in_specs, out_specs=out_specs, check_vma=False)
```

time: 108 us -> 98.9 us (0.916)
  the two profiles are of different devices: /device:TPU:32 before, /device:TPU:1 now
where the time goes in v2:
time: 98.9 us; the launch traced here: 98.5 us
  blocking collectives  92.8 us (94%)
  Pallas kernels  3.04 us (3%)
  local copies, waits for them, and re-layouts  1.88 us (2%)
    all_to_all x6, blocking collectives, exchange(): return lax.all_to_all(parts, axes, 0, 0, tiled=True)  92.8 us
    pallas_call x7, Pallas kernels, call(): pl.pallas_call(kernel, out_shape=out, in_specs=[pl.BlockSpec(memory_space...  3.04 us

profile of v2, /device:TPU:1, one launch (start us, length us, event | category | flops | bytes accessed | tf_op | source)
XLA Modules:
  0.0 98.5 jit_solution(1890248964441866769)
XLA Ops:
  0.6 0.0 copy-start.1
  0.6 0.1 pad_add_fusion.place
  0.7 0.6 copy-done.1
  1.3 0.0 copy-start
  1.4 1.2 %copy-done = bf16[256,2048]{1,0:T(8,128)(2,1)S(1)} copy-done((bf16[256,2048]{1,0:T(8,128)(2,1)S(1)}, bf16[256,2048]{1,0:T(8,128)(2,1)}, u32[]{:S(2)}) %copy-start) | copy-done | bytes 1048600
  2.6 0.9 pick.1
  3.5 34.1 %all_to_all.30.columns = bf16[64,8,128]{2,1,0:T(8,128)(2,1)S(1)} all-to-all(bf16[64,8,128]{2,1,0:T(8,128)(2,1)S(1)} %get-tuple-element.12), channel_id=1, replica_groups=mesh['zh'=8,'zl'=2,'y'=4,'x'=4,'c'=2] {'zh','zl','y'}, dimensions={0} | all-to-all | bytes 262144 | tf_op jit(solution)/shard_map/columns/all_to_all | solution.py:45
  37.6 0.6 project.1
  38.2 0.0 copy-start.2
  38.2 14.3 %all_to_all.31.both = bf16[8,64,256]{2,1,0:T(8,128)(2,1)S(1)} all-to-all(bf16[8,64,256]{2,1,0:T(8,128)(2,1)S(1)} %project.1), channel_id=1, replica_groups=mesh['zh'=8,'zl'=2,'y'=4,'x'=4,'c'=2] {'x','c'}, dimensions={0} | all-to-all | bytes 524288 | tf_op jit(solution)/shard_map/ranks/all_to_all | solution.py:45
  52.4 0.0 copy-done.2
  52.4 0.2 low.1
  52.6 0.0 copy-start.4
  52.7 0.0 copy-start.5
  52.7 8.0 %all_to_all.32.parts = f32[8,32,128]{2,1,0:T(8,128)S(1)} all-to-all(f32[8,32,128]{2,1,0:T(8,128)S(1)} %low.1), channel_id=1, replica_groups=mesh['zh'=8,'zl'=2,'y'=4,'x'=4,'c'=2] {'zl','y'}, dimensions={0} | all-to-all | bytes 262144 | tf_op jit(solution)/shard_map/near_sum/all_to_all | solution.py:45
  60.6 0.0 copy-done.4
  60.6 0.0 copy-done.5
  60.7 16.1 %all_to_all.33.parts = f32[8,40,128]{2,1,0:T(8,128)S(1)} all-to-all(f32[8,40,128]{2,1,0:T(8,128)S(1)} %sum_near.1), channel_id=1, replica_groups=mesh['zh'=8,'zl'=2,'y'=4,'x'=4,'c'=2] {'zh'}, dimensions={0} | all-to-all | bytes 327680 | tf_op jit(solution)/shard_map/far_sum/all_to_all | solution.py:45
  76.7 0.6 moments.1
  77.3 7.8 %all_to_all.34.parts = f32[8,32,128]{2,1,0:T(8,128)S(1)} all-to-all(f32[8,32,128]{2,1,0:T(8,128)S(1)} %get-tuple-element.13), channel_id=1, replica_groups=mesh['zh'=8,'zl'=2,'y'=4,'x'=4,'c'=2] {'zl','y'}, dimensions={0} | all-to-all | bytes 262144 | tf_op jit(solution)/shard_map/updates/all_to_all | solution.py:45
  85.2 0.2 apply.1
  85.3 12.5 %all_to_all.35.squares = f32[8,1,128]{2,1,0:T(1,128)S(1)} all-to-all(f32[8,1,128]{2,1,0:T(1,128)S(1)} %get-tuple-element.14.own), channel_id=1, replica_groups=mesh['zh'=8,'zl'=2,'y'=4,'x'=4,'c'=2] {'x','c'}, dimensions={0} | all-to-all | bytes 8192 | tf_op jit(solution)/shard_map/squares/all_to_all | solution.py:45
  97.8 0.0 copy-done.3
  97.8 0.6 scale.1
  (2 shorter events, 0.0 us)
Async XLA Ops:
  0.6 0.7 copy-start.1
  1.3 1.2 %copy-start = (bf16[256,2048]{1,0:T(8,128)(2,1)S(1)}, bf16[256,2048]{1,0:T(8,128)(2,1)}, u32[]{:S(2)}) copy-start(bf16[256,2048]{1,0:T(8,128)(2,1)} %inputs.1) | copy-start | bytes 3145732
  38.2 14.3 %copy-start.2 = (bf16[256,128]{1,0:T(8,128)(2,1)S(1)}, bf16[256,128]{1,0:T(8,128)(2,1)}, u32[]{:S(2)}) copy-start(bf16[256,128]{1,0:T(8,128)(2,1)} %cot.1) | copy-start | bytes 196612
  52.6 8.0 %copy-start.4 = (f32[4,128]{1,0:T(4,128)S(1)}, f32[4,128]{1,0:T(4,128)}, u32[]{:S(2)}) copy-start(f32[4,128]{1,0:T(4,128)} %first.1) | copy-start | bytes 6148
  52.7 8.0 %copy-start.5 = (f32[4,128]{1,0:T(4,128)S(1)}, f32[4,128]{1,0:T(4,128)}, u32[]{:S(2)}) copy-start(f32[4,128]{1,0:T(4,128)} %second.1) | copy-start | bytes 6148
  85.2 12.7 %copy-start.3 = (f32[32,128]{1,0:T(8,128)S(1)}, f32[32,128]{1,0:T(8,128)}, u32[]{:S(2)}) copy-start(f32[32,128]{1,0:T(8,128)} %master.1) | copy-start | bytes 49156

commit v3 on v2

--- a/solution.py
+++ b/solution.py
@@ -16,6 +16,12 @@
 GROUPS = ZL * NY
 PER = RANK // GROUPS
 OWN = PER // ZH
+FIRST_ROWS = 46
+FIRST_ZH = 5
+FIRST_RANKS = 5
+FIRST_SUM = 6
+FIRST_UPDATES = 6
+FIRST_SQUARES = 5
 
 F32 = jnp.float32
 BF16 = jnp.bfloat16
@@ -40,33 +46,39 @@
     )(*scalars, *operands)
 
 
-def exchange(parts, axes, name):
+def exchange(parts, axes, name, first=0):
+    count = parts.shape[0]
+    groups = [[(first + i) % count for i in range(count)]] if first else None
     with jax.named_scope(name):
-        return lax.all_to_all(parts, axes, 0, 0, tiled=True)
+        return lax.all_to_all(parts, axes, 0, 0, axis_index_groups=groups, tiled=True)
+
+
+def in_turn(blocks, first):
+    count = len(blocks)
+    return [blocks[(i - first) % count] for i in range(count)]
 
 
 def copies(block, count):
     return jnp.broadcast_to(block[None], (count, *block.shape))
 
 
-def pick_kernel(place, inputs, basis, out, held, rows, sems):
-    near = pltpu.make_async_copy(basis, rows, sems.at[0])
-    far = pltpu.make_async_copy(inputs, held, sems.at[1])
-    near.start()
-    far.start()
+def pick_kernel(place, inputs, basis, out, held, sem):
+    fetch = pltpu.make_async_copy(inputs, held, sem)
+    fetch.start()
     rank = lax.broadcasted_iota(jnp.int32, (RANK, PER), 0)
     slot = lax.broadcasted_iota(jnp.int32, (RANK, PER), 1)
     wanted = (slot // OWN) * PER + OWN * place[0] + slot % OWN
     chosen = (rank == wanted).astype(F32).astype(BF16)
-    near.wait()
-    mine = jnp.dot(rows[...], chosen, preferred_element_type=F32)
+    mine = jnp.dot(basis[...], chosen, preferred_element_type=F32)
     wide = jnp.concatenate([mine[8 * q : 8 * q + 8] for q in range(4)], axis=1)
     out[...] = copies(wide.astype(BF16), out.shape[0])
-    far.wait()
+    fetch.wait()
 
 
 def project_kernel(inputs, columns, out):
     got = columns[...].astype(F32)
+    if FIRST_ROWS:
+        got = jnp.concatenate([got[-FIRST_ROWS:], got[:-FIRST_ROWS]], axis=0)
     basis = jnp.concatenate([got[:, :, PER * q : PER * q + PER] for q in range(4)], axis=1)
     basis = basis.reshape(inputs.shape[1], PER).astype(BF16)
     low = jnp.dot(inputs[...], basis, preferred_element_type=F32)
@@ -79,7 +91,9 @@
 def low_kernel(both, cot, out):
     low = both[...].reshape(GROUPS * 2 * PER, both.shape[2])
     low = jnp.dot(low, cot[...], preferred_element_type=F32).reshape(GROUPS, 2 * PER, DQK)
-    out[...] = low[:, :PER] + low[:, PER:]
+    low = low[:, :PER] + low[:, PER:]
+    for g in range(GROUPS):
+        out[(g - FIRST_SUM) % GROUPS] = low[(g - FIRST_RANKS) % GROUPS]
 
 
 def sum_kernel(parts, first, second, out):
@@ -90,8 +104,10 @@
 
 def moments_kernel(place, parts, out, first_own, second_own, fn, sn):
     low = jnp.sum(parts[:, :PER, :], axis=0)
-    first = jnp.concatenate([parts[z, PER : PER + OWN, :] for z in range(ZH)], axis=0)
-    second = jnp.concatenate([parts[z, PER + OWN : PER + 2 * OWN, :] for z in range(ZH)], axis=0)
+    first = [parts[z, PER : PER + OWN, :] for z in range(ZH)]
+    first = jnp.concatenate(in_turn(first, FIRST_ZH), axis=0)
+    second = [parts[z, PER + OWN : PER + 2 * OWN, :] for z in range(ZH)]
+    second = jnp.concatenate(in_turn(second, FIRST_ZH), axis=0)
     first_new = 0.8 * first + 0.2 * low
     second_new = 0.9 * second + 0.1 * low * low
     fn[...] = first_new
@@ -104,7 +120,12 @@
 
 def apply_kernel(parts, basis, squares_out, step_out):
     update = jnp.concatenate(
-        [parts[g, OWN * z : OWN * (z + 1), :] for z in range(ZH) for g in range(GROUPS)], axis=0
+        [
+            parts[(g - FIRST_UPDATES) % GROUPS, OWN * z : OWN * (z + 1), :]
+            for z in range(ZH)
+            for g in range(GROUPS)
+        ],
+        axis=0,
     )
     squares = jnp.sum(jnp.sum(update * update, axis=0, keepdims=True), axis=1, keepdims=True)
     squares_out[...] = jnp.broadcast_to(squares[None], squares_out.shape)
@@ -137,11 +158,12 @@
         (sds((ZH * GROUPS, 8, DQK), BF16), sds(inputs.shape, BF16)),
         (inputs, query_basis),
         (place,),
-        specs=[pl.BlockSpec(memory_space=pltpu.HBM)] * 2,
-        scratch=[pltpu.VMEM(query_basis.shape, BF16), pltpu.SemaphoreType.DMA((2,))],
+        specs=[pl.BlockSpec(memory_space=pltpu.HBM), *vmem(1)],
+        scratch=[pltpu.SemaphoreType.DMA],
+        limit=54000 << 10,
         name="pick",
     )
-    columns = exchange(columns, FS, "columns")
+    columns = exchange(columns, FS, "columns", FIRST_ROWS)
     both = call(
         project_kernel,
         sds((GROUPS, 2 * PER, tokens), BF16),
@@ -150,16 +172,16 @@
         limit=16 << 20,
         name="project",
     )
-    both = exchange(both, TP, "ranks")
+    both = exchange(both, TP, "ranks", FIRST_RANKS)
     low = call(low_kernel, sds((GROUPS, PER, DQK), F32), (both, query_cot), name="low")
-    low = exchange(low, NEAR, "near_sum")
+    low = exchange(low, NEAR, "near_sum", FIRST_SUM)
     low = call(
         sum_kernel,
         sds((ZH, PER + 2 * OWN, DQK), F32),
         (low, query_first, query_second),
         name="sum_near",
     )
-    low = exchange(low, "zh", "far_sum")
+    low = exchange(low, "zh", "far_sum", FIRST_ZH)
     update, first_new, second_new = call(
         moments_kernel,
         (sds((GROUPS, PER, DQK), F32), small, small),
@@ -168,14 +190,14 @@
         scratch=[pltpu.VMEM((PER, DQK), F32)] * 2,
         name="moments",
     )
-    update = exchange(update, NEAR, "updates")
+    update = exchange(update, NEAR, "updates", FIRST_UPDATES)
     squares, step = call(
         apply_kernel,
         (sds((HEADS, 1, DQK), F32), sds(query_master.shape, F32)),
         (update, query_basis),
         name="apply",
     )
-    heads = exchange(squares, TP, "squares")
+    heads = exchange(squares, TP, "squares", FIRST_SQUARES)
     step, first_new, second_new, copy = call(
         scale_kernel,
         (sds(query_master.shape, F32), small, small, sds(query_master.shape, BF16)),

time: 98.9 us -> 88 us (0.89)
  blocking collectives: 92.8 us -> 82.1 us
  local copies, waits for them, and re-layouts: 1.88 us -> 0.65 us
    all_to_all x6, blocking collectives: 92.8 us -> 82.1 us  [exchange(): lax.all_to_all(parts, axes, 0, 0, axis_index_groups=groups, tiled=True)]
    unnamed x12 -> x10, local copies, waits for them, and re-layouts: 1.88 us -> 0.65 us
where the time goes in v3:
time: 88 us; the launch traced here: 87.5 us
  blocking collectives  82.1 us (93%)
  Pallas kernels  3.94 us (4%)
    all_to_all x6, blocking collectives, exchange(): lax.all_to_all(parts, axes, 0, 0, axis_index_groups=groups, tiled=True)  82.1 us
    pallas_call x7, Pallas kernels, call(): pl.pallas_call(kernel, out_shape=out, in_specs=[pl.BlockSpec(memory_space...  3.94 us

profile of v3, /device:TPU:1, one launch (start us, length us, event | category | flops | bytes accessed | tf_op | source)
XLA Modules:
  0.0 87.5 jit_solution(11632054897179142907)
XLA Ops:
  0.6 0.0 copy-start
  0.6 0.1 pad_add_fusion.place
  0.7 0.6 copy-done
  1.3 1.8 %pick.1 = (bf16[64,8,128]{2,1,0:T(8,128)(2,1)S(1)}, bf16[256,2048]{1,0:T(8,128)(2,1)S(1)}) custom-call(s32[2]{0:T(128)S(1)} %pad_add_fusion.place, bf16[256,2048]{1,0:T(8,128)(2,1)} %inputs.1, bf16[32,256]{1,0:T(8,128)(2,1)S(1)} %copy-done), custom_call_target="tpu_custom_call" | custom-call | flops 200000 | bytes 1064960 | tf_op jit(solution)/shard_map/pick/pallas_call | solution.py:37
  3.1 28.1 %all_to_all.30.columns = bf16[64,8,128]{2,1,0:T(8,128)(2,1)S(1)} all-to-all(bf16[64,8,128]{2,1,0:T(8,128)(2,1)S(1)} %get-tuple-element.12), channel_id=1, replica_groups={{368,376,384,392,400,408,416,424,432,440,448,456,464,472,480,488,496,50..., dimensions={0} | all-to-all | bytes 262144 | tf_op jit(solution)/shard_map/columns/all_to_all | solution.py:53
  31.2 0.6 project.1
  31.8 0.0 copy-start.1
  31.8 10.2 %all_to_all.31.both = bf16[8,64,256]{2,1,0:T(8,128)(2,1)S(1)} all-to-all(bf16[8,64,256]{2,1,0:T(8,128)(2,1)S(1)} %project.1), channel_id=1, replica_groups={{5,6,7,0,1,2,3,4},{13,14,15,8,9,10,11,12},{21,22,23,16,17,18,19,20},{29..., dimensions={0} | all-to-all | bytes 524288 | tf_op jit(solution)/shard_map/ranks/all_to_all | solution.py:53
  42.0 0.0 copy-done.1
  42.0 0.2 low.1
  42.2 0.0 copy-start.3
  42.3 0.0 copy-start.4
  42.3 8.3 %all_to_all.32.parts = f32[8,32,128]{2,1,0:T(8,128)S(1)} all-to-all(f32[8,32,128]{2,1,0:T(8,128)S(1)} %low.1), channel_id=1, replica_groups={{48,56,0,8,16,24,32,40},{49,57,1,9,17,25,33,41},{50,58,2,10,18,26,34,42..., dimensions={0} | all-to-all | bytes 262144 | tf_op jit(solution)/shard_map/near_sum/all_to_all | solution.py:53
  50.5 0.0 copy-done.3
  50.5 0.0 copy-done.4
  50.6 15.6 %all_to_all.33.parts = f32[8,40,128]{2,1,0:T(8,128)S(1)} all-to-all(f32[8,40,128]{2,1,0:T(8,128)S(1)} %sum_near.1), channel_id=1, replica_groups={{320,384,448,0,64,128,192,256},{321,385,449,1,65,129,193,257},{322,386,..., dimensions={0} | all-to-all | bytes 327680 | tf_op jit(solution)/shard_map/far_sum/all_to_all | solution.py:53
  66.1 0.6 moments.1
  66.7 8.8 %all_to_all.34.parts = f32[8,32,128]{2,1,0:T(8,128)S(1)} all-to-all(f32[8,32,128]{2,1,0:T(8,128)S(1)} %get-tuple-element.13), channel_id=1, replica_groups={{48,56,0,8,16,24,32,40},{49,57,1,9,17,25,33,41},{50,58,2,10,18,26,34,42..., dimensions={0} | all-to-all | bytes 262144 | tf_op jit(solution)/shard_map/updates/all_to_all | solution.py:53
  75.5 0.0 copy-start.2
  75.5 0.2 apply.1
  75.7 11.2 %all_to_all.35.squares = f32[8,1,128]{2,1,0:T(1,128)S(1)} all-to-all(f32[8,1,128]{2,1,0:T(1,128)S(1)} %get-tuple-element.14.own), channel_id=1, replica_groups={{5,6,7,0,1,2,3,4},{13,14,15,8,9,10,11,12},{21,22,23,16,17,18,19,20},{29..., dimensions={0} | all-to-all | bytes 8192 | tf_op jit(solution)/shard_map/squares/all_to_all | solution.py:53
  86.9 0.0 copy-done.2
  86.9 0.6 scale.1
  (1 shorter events, 0.0 us)
Async XLA Ops:
  0.6 0.7 copy-start
  31.8 10.2 %copy-start.1 = (bf16[256,128]{1,0:T(8,128)(2,1)S(1)}, bf16[256,128]{1,0:T(8,128)(2,1)}, u32[]{:S(2)}) copy-start(bf16[256,128]{1,0:T(8,128)(2,1)} %cot.1) | copy-start | bytes 196612
  42.2 8.3 %copy-start.3 = (f32[4,128]{1,0:T(4,128)S(1)}, f32[4,128]{1,0:T(4,128)}, u32[]{:S(2)}) copy-start(f32[4,128]{1,0:T(4,128)} %first.1) | copy-start | bytes 6148
  42.3 8.3 %copy-start.4 = (f32[4,128]{1,0:T(4,128)S(1)}, f32[4,128]{1,0:T(4,128)}, u32[]{:S(2)}) copy-start(f32[4,128]{1,0:T(4,128)} %second.1) | copy-start | bytes 6148
  75.5 11.4 %copy-start.2 = (f32[32,128]{1,0:T(8,128)S(1)}, f32[32,128]{1,0:T(8,128)}, u32[]{:S(2)}) copy-start(f32[32,128]{1,0:T(8,128)} %master.1) | copy-start | bytes 49156

commit v4 on v3

--- a/solution.py
+++ b/solution.py
@@ -16,6 +16,7 @@
 GROUPS = ZL * NY
 PER = RANK // GROUPS
 OWN = PER // ZH
+FETCHES = 2
 FIRST_ROWS = 46
 FIRST_ZH = 5
 FIRST_RANKS = 5
@@ -62,30 +63,39 @@
     return jnp.broadcast_to(block[None], (count, *block.shape))
 
 
-def pick_kernel(place, inputs, basis, out, held, sem):
-    fetch = pltpu.make_async_copy(inputs, held, sem)
-    fetch.start()
+def pick_kernel(inputs, basis, out, held, rows, sems):
+    near = pltpu.make_async_copy(basis, rows, sems.at[0])
+    near.start()
+    fetches = []
+    for i in range(FETCHES):
+        part = pl.ds(i * (held.shape[0] // FETCHES), held.shape[0] // FETCHES)
+        fetches.append(pltpu.make_async_copy(inputs.at[part], held.at[part], sems.at[1 + i]))
+    for fetch in fetches:
+        fetch.start()
     rank = lax.broadcasted_iota(jnp.int32, (RANK, PER), 0)
     slot = lax.broadcasted_iota(jnp.int32, (RANK, PER), 1)
-    wanted = (slot // OWN) * PER + OWN * place[0] + slot % OWN
+    wanted = (slot // OWN) * PER + OWN * lax.axis_index(TP) + slot % OWN
     chosen = (rank == wanted).astype(F32).astype(BF16)
-    mine = jnp.dot(basis[...], chosen, preferred_element_type=F32)
+    near.wait()
+    mine = jnp.dot(rows[...], chosen, preferred_element_type=F32)
     wide = jnp.concatenate([mine[8 * q : 8 * q + 8] for q in range(4)], axis=1)
     out[...] = copies(wide.astype(BF16), out.shape[0])
-    fetch.wait()
+    for fetch in fetches:
+        fetch.wait()
 
 
 def project_kernel(inputs, columns, out):
     got = columns[...].astype(F32)
     if FIRST_ROWS:
         got = jnp.concatenate([got[-FIRST_ROWS:], got[:-FIRST_ROWS]], axis=0)
-    basis = jnp.concatenate([got[:, :, PER * q : PER * q + PER] for q in range(4)], axis=1)
-    basis = basis.reshape(inputs.shape[1], PER).astype(BF16)
-    low = jnp.dot(inputs[...], basis, preferred_element_type=F32)
+    lane = lax.broadcasted_iota(jnp.int32, got.shape, 2) // PER
+    basis = jnp.concatenate([jnp.where(lane == q, got, 0.0) for q in range(4)], axis=1)
+    basis = basis.reshape(inputs.shape[1], DQK).astype(BF16)
+    low = jnp.dot(inputs[...], basis, preferred_element_type=F32).T
+    low = (low[:PER] + low[PER : 2 * PER]) + (low[2 * PER : 3 * PER] + low[3 * PER :])
     high = low.astype(BF16)
     rest = (low - high.astype(F32)).astype(BF16)
-    both = jnp.concatenate([high.astype(F32).T, rest.astype(F32).T], axis=0).astype(BF16)
-    out[...] = copies(both, out.shape[0])
+    out[...] = copies(jnp.concatenate([high, rest], axis=0), out.shape[0])
 
 
 def low_kernel(both, cot, out):
@@ -102,7 +112,7 @@
     out[:, PER:, :] = copies(pair, ZH)
 
 
-def moments_kernel(place, parts, out, first_own, second_own, fn, sn):
+def moments_kernel(parts, out, first_own, second_own, fn, sn):
     low = jnp.sum(parts[:, :PER, :], axis=0)
     first = [parts[z, PER : PER + OWN, :] for z in range(ZH)]
     first = jnp.concatenate(in_turn(first, FIRST_ZH), axis=0)
@@ -113,7 +123,7 @@
     fn[...] = first_new
     sn[...] = second_new
     out[...] = copies(first_new / jnp.sqrt(second_new), GROUPS)
-    rows = pl.ds(OWN * place[1], OWN)
+    rows = pl.ds(OWN * lax.axis_index("zh"), OWN)
     first_own[...] = fn[rows, :]
     second_own[...] = sn[rows, :]
 
@@ -151,16 +161,14 @@
 
 def body(inputs, query_cot, query_basis, query_master, query_first, query_second):
     sds = jax.ShapeDtypeStruct
-    place = jnp.stack([lax.axis_index(TP), lax.axis_index("zh")]).astype(jnp.int32)
     tokens, small = inputs.shape[0], sds(query_first.shape, F32)
     columns, held = call(
         pick_kernel,
         (sds((ZH * GROUPS, 8, DQK), BF16), sds(inputs.shape, BF16)),
-        (inputs, query_basis),
-        (place,),
-        specs=[pl.BlockSpec(memory_space=pltpu.HBM), *vmem(1)],
-        scratch=[pltpu.SemaphoreType.DMA],
-        limit=54000 << 10,
+        [pltpu.with_memory_space_constraint(a, pltpu.HBM) for a in (inputs, query_basis)],
+        specs=[pl.BlockSpec(memory_space=pltpu.HBM)] * 2,
+        scratch=[pltpu.VMEM(query_basis.shape, BF16), pltpu.SemaphoreType.DMA((1 + FETCHES,))],
+        limit=4 << 20,
         name="pick",
     )
     columns = exchange(columns, FS, "columns", FIRST_ROWS)
@@ -186,7 +194,6 @@
         moments_kernel,
         (sds((GROUPS, PER, DQK), F32), small, small),
         (low,),
-        (place,),
         scratch=[pltpu.VMEM((PER, DQK), F32)] * 2,
         name="moments",
     )

time: 88 us -> 86.1 us (0.978)
  Pallas kernels: 3.94 us -> 2.81 us
    pallas_call x7, Pallas kernels: 3.94 us -> 2.81 us  [call(): pl.pallas_call(kernel, out_shape=out, in_specs=[pl.BlockSpec(memory_space...]
where the time goes in v4:
time: 86.1 us; the launch traced here: 85.7 us
  blocking collectives  82.1 us (95%)
  Pallas kernels  2.81 us (3%)
    all_to_all x6, blocking collectives, exchange(): lax.all_to_all(parts, axes, 0, 0, axis_index_groups=groups, tiled=True)  82.1 us
    pallas_call x7, Pallas kernels, call(): pl.pallas_call(kernel, out_shape=out, in_specs=[pl.BlockSpec(memory_space...  2.81 us

profile of v4, /device:TPU:1, one launch (start us, length us, event | category | flops | bytes accessed | tf_op | source)
XLA Modules:
  0.0 85.7 jit_solution(15680437644243157117)
XLA Ops:
  0.6 1.2 %pick.1 = (bf16[64,8,128]{2,1,0:T(8,128)(2,1)S(1)}, bf16[256,2048]{1,0:T(8,128)(2,1)S(1)}) custom-call(bf16[256,2048]{1,0:T(8,128)(2,1)} %inputs.1, bf16[32,256]{1,0:T(8,128)(2,1)} %basis.3), custom_call_target="tpu_custom_call" | custom-call | flops 200000 | bytes 1064960 | tf_op jit(solution)/shard_map/pick/pallas_call | solution.py:38
  1.9 28.1 %all_to_all.30.columns = bf16[64,8,128]{2,1,0:T(8,128)(2,1)S(1)} all-to-all(bf16[64,8,128]{2,1,0:T(8,128)(2,1)S(1)} %get-tuple-element.12), channel_id=1, replica_groups={{368,376,384,392,400,408,416,424,432,440,448,456,464,472,480,488,496,50..., dimensions={0} | all-to-all | bytes 262144 | tf_op jit(solution)/shard_map/columns/all_to_all | solution.py:54
  30.0 0.5 project.1
  30.5 0.0 copy-start.1
  30.5 10.2 %all_to_all.31.both = bf16[8,64,256]{2,1,0:T(8,128)(2,1)S(1)} all-to-all(bf16[8,64,256]{2,1,0:T(8,128)(2,1)S(1)} %project.1), channel_id=1, replica_groups={{5,6,7,0,1,2,3,4},{13,14,15,8,9,10,11,12},{21,22,23,16,17,18,19,20},{29..., dimensions={0} | all-to-all | bytes 524288 | tf_op jit(solution)/shard_map/ranks/all_to_all | solution.py:54
  40.7 0.0 copy-done.1
  40.7 0.2 low.1
  40.9 0.0 copy-start.3
  40.9 0.0 copy-start.4
  41.0 8.3 %all_to_all.32.parts = f32[8,32,128]{2,1,0:T(8,128)S(1)} all-to-all(f32[8,32,128]{2,1,0:T(8,128)S(1)} %low.1), channel_id=1, replica_groups={{48,56,0,8,16,24,32,40},{49,57,1,9,17,25,33,41},{50,58,2,10,18,26,34,42..., dimensions={0} | all-to-all | bytes 262144 | tf_op jit(solution)/shard_map/near_sum/all_to_all | solution.py:54
  49.2 0.0 copy-done.3
  49.2 0.0 copy-done.4
  49.2 15.6 %all_to_all.33.parts = f32[8,40,128]{2,1,0:T(8,128)S(1)} all-to-all(f32[8,40,128]{2,1,0:T(8,128)S(1)} %sum_near.1), channel_id=1, replica_groups={{320,384,448,0,64,128,192,256},{321,385,449,1,65,129,193,257},{322,386,..., dimensions={0} | all-to-all | bytes 327680 | tf_op jit(solution)/shard_map/far_sum/all_to_all | solution.py:54
  64.9 0.0 copy-start
  64.9 8.8 %all_to_all.34.parts = f32[8,32,128]{2,1,0:T(8,128)S(1)} all-to-all(f32[8,32,128]{2,1,0:T(8,128)S(1)} %get-tuple-element.13), channel_id=1, replica_groups={{48,56,0,8,16,24,32,40},{49,57,1,9,17,25,33,41},{50,58,2,10,18,26,34,42..., dimensions={0} | all-to-all | bytes 262144 | tf_op jit(solution)/shard_map/updates/all_to_all | solution.py:54
  73.7 0.0 copy-done
  73.7 0.0 copy-start.2
  73.7 0.2 apply.1
  73.8 11.2 %all_to_all.35.squares = f32[8,1,128]{2,1,0:T(1,128)S(1)} all-to-all(f32[8,1,128]{2,1,0:T(1,128)S(1)} %get-tuple-element.14.own), channel_id=1, replica_groups={{5,6,7,0,1,2,3,4},{13,14,15,8,9,10,11,12},{21,22,23,16,17,18,19,20},{29..., dimensions={0} | all-to-all | bytes 8192 | tf_op jit(solution)/shard_map/squares/all_to_all | solution.py:54
  85.0 0.0 copy-done.2
  85.0 0.6 scale.1
  (2 shorter events, 0.1 us)
Async XLA Ops:
  30.5 10.2 %copy-start.1 = (bf16[256,128]{1,0:T(8,128)(2,1)S(1)}, bf16[256,128]{1,0:T(8,128)(2,1)}, u32[]{:S(2)}) copy-start(bf16[256,128]{1,0:T(8,128)(2,1)} %cot.1) | copy-start | bytes 196612
  40.9 8.3 %copy-start.3 = (f32[4,128]{1,0:T(4,128)S(1)}, f32[4,128]{1,0:T(4,128)}, u32[]{:S(2)}) copy-start(f32[4,128]{1,0:T(4,128)} %first.1) | copy-start | bytes 6148
  40.9 8.3 %copy-start.4 = (f32[4,128]{1,0:T(4,128)S(1)}, f32[4,128]{1,0:T(4,128)}, u32[]{:S(2)}) copy-start(f32[4,128]{1,0:T(4,128)} %second.1) | copy-start | bytes 6148
  64.9 8.8 %copy-start = (bf16[32,256]{1,0:T(8,128)(2,1)S(1)}, bf16[32,256]{1,0:T(8,128)(2,1)}, u32[]{:S(2)}) copy-start(bf16[32,256]{1,0:T(8,128)(2,1)} %basis.3) | copy-start | bytes 49156
  73.7 11.4 %copy-start.2 = (f32[32,128]{1,0:T(8,128)S(1)}, f32[32,128]{1,0:T(8,128)}, u32[]{:S(2)}) copy-start(f32[32,128]{1,0:T(8,128)} %master.1) | copy-start | bytes 49156

commit v5 on v4

--- a/solution.py
+++ b/solution.py
@@ -18,7 +18,7 @@
 OWN = PER // ZH
 FETCHES = 2
 FIRST_ROWS = 46
-FIRST_ZH = 5
+FIRST_ZH = (5, 4)
 FIRST_RANKS = 5
 FIRST_SUM = 6
 FIRST_UPDATES = 6
@@ -52,11 +52,6 @@
     groups = [[(first + i) % count for i in range(count)]] if first else None
     with jax.named_scope(name):
         return lax.all_to_all(parts, axes, 0, 0, axis_index_groups=groups, tiled=True)
-
-
-def in_turn(blocks, first):
-    count = len(blocks)
-    return [blocks[(i - first) % count] for i in range(count)]
 
 
 def copies(block, count):
@@ -114,10 +109,10 @@
 
 def moments_kernel(parts, out, first_own, second_own, fn, sn):
     low = jnp.sum(parts[:, :PER, :], axis=0)
-    first = [parts[z, PER : PER + OWN, :] for z in range(ZH)]
-    first = jnp.concatenate(in_turn(first, FIRST_ZH), axis=0)
-    second = [parts[z, PER + OWN : PER + 2 * OWN, :] for z in range(ZH)]
-    second = jnp.concatenate(in_turn(second, FIRST_ZH), axis=0)
+    start = jnp.where(lax.axis_index("zl") == 0, FIRST_ZH[0], FIRST_ZH[1])
+    turn = [lax.rem(z + ZH - start, ZH) for z in range(ZH)]
+    first = jnp.concatenate([parts[t, PER : PER + OWN, :] for t in turn], axis=0)
+    second = jnp.concatenate([parts[t, PER + OWN : PER + 2 * OWN, :] for t in turn], axis=0)
     first_new = 0.8 * first + 0.2 * low
     second_new = 0.9 * second + 0.1 * low * low
     fn[...] = first_new
@@ -189,7 +184,9 @@
         (low, query_first, query_second),
         name="sum_near",
     )
-    low = exchange(low, "zh", "far_sum", FIRST_ZH)
+    groups = [[(FIRST_ZH[b] + i) % ZH * ZL + b for i in range(ZH)] for b in range(ZL)]
+    with jax.named_scope("far_sum"):
+        low = lax.all_to_all(low, ("zh", "zl"), 0, 0, axis_index_groups=groups, tiled=True)
     update, first_new, second_new = call(
         moments_kernel,
         (sds((GROUPS, PER, DQK), F32), small, small),

time: 86.1 us -> 85.6 us (level)
    all_to_all x6 -> x5, blocking collectives: 82.1 us -> 66.1 us  [exchange(): lax.all_to_all(parts, axes, 0, 0, axis_index_groups=groups, tiled=True)]
    all_to_all x0 -> x1, blocking collectives: none -> 15.4 us  [body(): lax.all_to_all(low, ('zh', 'zl'), 0, 0, axis_index_groups=groups, tiled=T...]
where the time goes in v5:
time: 85.6 us; the launch traced here: 85.1 us
  blocking collectives  81.6 us (95%)
  Pallas kernels  2.82 us (3%)
    all_to_all x5, blocking collectives, exchange(): lax.all_to_all(parts, axes, 0, 0, axis_index_groups=groups, tiled=True)  66.1 us
    all_to_all x1, blocking collectives, body(): lax.all_to_all(low, ('zh', 'zl'), 0, 0, axis_index_groups=groups, tiled=T...  15.4 us
    pallas_call x7, Pallas kernels, call(): pl.pallas_call(kernel, out_shape=out, in_specs=[pl.BlockSpec(memory_space...  2.82 us

profile of v5, /device:TPU:1, one launch (start us, length us, event | category | flops | bytes accessed | tf_op | source)
XLA Modules:
  0.0 85.1 jit_solution(4326970783457868415)
XLA Ops:
  0.6 1.2 %pick.1 = (bf16[64,8,128]{2,1,0:T(8,128)(2,1)S(1)}, bf16[256,2048]{1,0:T(8,128)(2,1)S(1)}) custom-call(bf16[256,2048]{1,0:T(8,128)(2,1)} %inputs.1, bf16[32,256]{1,0:T(8,128)(2,1)} %basis.3), custom_call_target="tpu_custom_call" | custom-call | flops 200000 | bytes 1064960 | tf_op jit(solution)/shard_map/pick/pallas_call | solution.py:38
  1.9 28.1 %all_to_all.30.columns = bf16[64,8,128]{2,1,0:T(8,128)(2,1)S(1)} all-to-all(bf16[64,8,128]{2,1,0:T(8,128)(2,1)S(1)} %get-tuple-element.12), channel_id=1, replica_groups={{368,376,384,392,400,408,416,424,432,440,448,456,464,472,480,488,496,50..., dimensions={0} | all-to-all | bytes 262144 | tf_op jit(solution)/shard_map/columns/all_to_all | solution.py:54
  30.0 0.5 project.1
  30.5 0.0 copy-start.1
  30.5 10.2 %all_to_all.31.both = bf16[8,64,256]{2,1,0:T(8,128)(2,1)S(1)} all-to-all(bf16[8,64,256]{2,1,0:T(8,128)(2,1)S(1)} %project.1), channel_id=1, replica_groups={{5,6,7,0,1,2,3,4},{13,14,15,8,9,10,11,12},{21,22,23,16,17,18,19,20},{29..., dimensions={0} | all-to-all | bytes 524288 | tf_op jit(solution)/shard_map/ranks/all_to_all | solution.py:54
  40.7 0.0 copy-done.1
  40.7 0.2 low.1
  40.9 0.0 copy-start.3
  40.9 0.0 copy-start.4
  41.0 8.3 %all_to_all.32.parts = f32[8,32,128]{2,1,0:T(8,128)S(1)} all-to-all(f32[8,32,128]{2,1,0:T(8,128)S(1)} %low.1), channel_id=1, replica_groups={{48,56,0,8,16,24,32,40},{49,57,1,9,17,25,33,41},{50,58,2,10,18,26,34,42..., dimensions={0} | all-to-all | bytes 262144 | tf_op jit(solution)/shard_map/near_sum/all_to_all | solution.py:54
  49.2 0.0 copy-done.3
  49.2 0.0 copy-done.4
  49.2 15.4 %all_to_all.33.parts = f32[8,40,128]{2,1,0:T(8,128)S(1)} all-to-all(f32[8,40,128]{2,1,0:T(8,128)S(1)} %sum_near.1), channel_id=1, replica_groups={{320,384,448,0,64,128,192,256},{288,352,416,480,32,96,160,224},{321,385..., dimensions={0} | all-to-all | bytes 327680 | tf_op jit(solution)/shard_map/far_sum/all_to_all | solution.py:189
  64.7 0.0 copy-start
  64.7 8.0 %all_to_all.34.parts = f32[8,32,128]{2,1,0:T(8,128)S(1)} all-to-all(f32[8,32,128]{2,1,0:T(8,128)S(1)} %get-tuple-element.13), channel_id=1, replica_groups={{48,56,0,8,16,24,32,40},{49,57,1,9,17,25,33,41},{50,58,2,10,18,26,34,42..., dimensions={0} | all-to-all | bytes 262144 | tf_op jit(solution)/shard_map/updates/all_to_all | solution.py:54
  72.7 0.0 copy-done
  72.7 0.0 copy-start.2
  72.7 0.2 apply.1
  72.9 11.6 %all_to_all.35.squares = f32[8,1,128]{2,1,0:T(1,128)S(1)} all-to-all(f32[8,1,128]{2,1,0:T(1,128)S(1)} %get-tuple-element.14.own), channel_id=1, replica_groups={{5,6,7,0,1,2,3,4},{13,14,15,8,9,10,11,12},{21,22,23,16,17,18,19,20},{29..., dimensions={0} | all-to-all | bytes 8192 | tf_op jit(solution)/shard_map/squares/all_to_all | solution.py:54
  84.5 0.0 copy-done.2
  84.5 0.6 scale.1
  (2 shorter events, 0.1 us)
Async XLA Ops:
  30.5 10.2 %copy-start.1 = (bf16[256,128]{1,0:T(8,128)(2,1)S(1)}, bf16[256,128]{1,0:T(8,128)(2,1)}, u32[]{:S(2)}) copy-start(bf16[256,128]{1,0:T(8,128)(2,1)} %cot.1) | copy-start | bytes 196612
  40.9 8.3 %copy-start.3 = (f32[4,128]{1,0:T(4,128)S(1)}, f32[4,128]{1,0:T(4,128)}, u32[]{:S(2)}) copy-start(f32[4,128]{1,0:T(4,128)} %first.1) | copy-start | bytes 6148
  40.9 8.3 %copy-start.4 = (f32[4,128]{1,0:T(4,128)S(1)}, f32[4,128]{1,0:T(4,128)}, u32[]{:S(2)}) copy-start(f32[4,128]{1,0:T(4,128)} %second.1) | copy-start | bytes 6148
  64.7 8.0 %copy-start = (bf16[32,256]{1,0:T(8,128)(2,1)S(1)}, bf16[32,256]{1,0:T(8,128)(2,1)}, u32[]{:S(2)}) copy-start(bf16[32,256]{1,0:T(8,128)(2,1)} %basis.3) | copy-start | bytes 49156
  72.7 11.8 %copy-start.2 = (f32[32,128]{1,0:T(8,128)S(1)}, f32[32,128]{1,0:T(8,128)}, u32[]{:S(2)}) copy-start(f32[32,128]{1,0:T(8,128)} %master.1) | copy-start | bytes 49156

commit v6 on v5

--- a/solution.py
+++ b/solution.py
@@ -17,7 +17,7 @@
 PER = RANK // GROUPS
 OWN = PER // ZH
 FETCHES = 2
-FIRST_ROWS = 46
+FIRST_ROWS = 47
 FIRST_ZH = (5, 4)
 FIRST_RANKS = 5
 FIRST_SUM = 6

time: 85.6 us -> 85.4 us (level)
  no operation moved by 1% of the time
where the time goes in v6:
time: 85.4 us; the launch traced here: 85 us
  blocking collectives  81.4 us (95%)
  Pallas kernels  2.82 us (3%)
    all_to_all x5, blocking collectives, exchange(): lax.all_to_all(parts, axes, 0, 0, axis_index_groups=groups, tiled=True)  65.5 us
    all_to_all x1, blocking collectives, body(): lax.all_to_all(low, ('zh', 'zl'), 0, 0, axis_index_groups=groups, tiled=T...  15.9 us
    pallas_call x7, Pallas kernels, call(): pl.pallas_call(kernel, out_shape=out, in_specs=[pl.BlockSpec(memory_space...  2.82 us

profile of v6, /device:TPU:1, one launch (start us, length us, event | category | flops | bytes accessed | tf_op | source)
XLA Modules:
  0.0 85.0 jit_solution(1283501966945388470)
XLA Ops:
  0.6 1.2 %pick.1 = (bf16[64,8,128]{2,1,0:T(8,128)(2,1)S(1)}, bf16[256,2048]{1,0:T(8,128)(2,1)S(1)}) custom-call(bf16[256,2048]{1,0:T(8,128)(2,1)} %inputs.1, bf16[32,256]{1,0:T(8,128)(2,1)} %basis.3), custom_call_target="tpu_custom_call" | custom-call | flops 200000 | bytes 1064960 | tf_op jit(solution)/shard_map/pick/pallas_call | solution.py:38
  1.9 27.9 %all_to_all.30.columns = bf16[64,8,128]{2,1,0:T(8,128)(2,1)S(1)} all-to-all(bf16[64,8,128]{2,1,0:T(8,128)(2,1)S(1)} %get-tuple-element.12), channel_id=1, replica_groups={{376,384,392,400,408,416,424,432,440,448,456,464,472,480,488,496,504,0,..., dimensions={0} | all-to-all | bytes 262144 | tf_op jit(solution)/shard_map/columns/all_to_all | solution.py:54
  29.7 0.5 project.1
  30.2 0.0 copy-start.1
  30.3 10.9 %all_to_all.31.both = bf16[8,64,256]{2,1,0:T(8,128)(2,1)S(1)} all-to-all(bf16[8,64,256]{2,1,0:T(8,128)(2,1)S(1)} %project.1), channel_id=1, replica_groups={{5,6,7,0,1,2,3,4},{13,14,15,8,9,10,11,12},{21,22,23,16,17,18,19,20},{29..., dimensions={0} | all-to-all | bytes 524288 | tf_op jit(solution)/shard_map/ranks/all_to_all | solution.py:54
  41.1 0.0 copy-done.1
  41.1 0.2 low.1
  41.3 0.0 copy-start.3
  41.3 0.0 copy-start.4
  41.4 7.6 %all_to_all.32.parts = f32[8,32,128]{2,1,0:T(8,128)S(1)} all-to-all(f32[8,32,128]{2,1,0:T(8,128)S(1)} %low.1), channel_id=1, replica_groups={{48,56,0,8,16,24,32,40},{49,57,1,9,17,25,33,41},{50,58,2,10,18,26,34,42..., dimensions={0} | all-to-all | bytes 262144 | tf_op jit(solution)/shard_map/near_sum/all_to_all | solution.py:54
  49.0 0.0 copy-done.3
  49.0 0.0 copy-done.4
  49.0 15.9 %all_to_all.33.parts = f32[8,40,128]{2,1,0:T(8,128)S(1)} all-to-all(f32[8,40,128]{2,1,0:T(8,128)S(1)} %sum_near.1), channel_id=1, replica_groups={{320,384,448,0,64,128,192,256},{288,352,416,480,32,96,160,224},{321,385..., dimensions={0} | all-to-all | bytes 327680 | tf_op jit(solution)/shard_map/far_sum/all_to_all | solution.py:189
  65.0 0.0 copy-start
  65.0 7.8 %all_to_all.34.parts = f32[8,32,128]{2,1,0:T(8,128)S(1)} all-to-all(f32[8,32,128]{2,1,0:T(8,128)S(1)} %get-tuple-element.13), channel_id=1, replica_groups={{48,56,0,8,16,24,32,40},{49,57,1,9,17,25,33,41},{50,58,2,10,18,26,34,42..., dimensions={0} | all-to-all | bytes 262144 | tf_op jit(solution)/shard_map/updates/all_to_all | solution.py:54
  72.8 0.0 copy-done
  72.8 0.0 copy-start.2
  72.8 0.2 apply.1
  73.0 11.3 %all_to_all.35.squares = f32[8,1,128]{2,1,0:T(1,128)S(1)} all-to-all(f32[8,1,128]{2,1,0:T(1,128)S(1)} %get-tuple-element.14.own), channel_id=1, replica_groups={{5,6,7,0,1,2,3,4},{13,14,15,8,9,10,11,12},{21,22,23,16,17,18,19,20},{29..., dimensions={0} | all-to-all | bytes 8192 | tf_op jit(solution)/shard_map/squares/all_to_all | solution.py:54
  84.3 0.0 copy-done.2
  84.3 0.6 scale.1
  (2 shorter events, 0.1 us)
Async XLA Ops:
  30.2 10.9 %copy-start.1 = (bf16[256,128]{1,0:T(8,128)(2,1)S(1)}, bf16[256,128]{1,0:T(8,128)(2,1)}, u32[]{:S(2)}) copy-start(bf16[256,128]{1,0:T(8,128)(2,1)} %cot.1) | copy-start | bytes 196612
  41.3 7.7 %copy-start.3 = (f32[4,128]{1,0:T(4,128)S(1)}, f32[4,128]{1,0:T(4,128)}, u32[]{:S(2)}) copy-start(f32[4,128]{1,0:T(4,128)} %first.1) | copy-start | bytes 6148
  41.3 7.6 %copy-start.4 = (f32[4,128]{1,0:T(4,128)S(1)}, f32[4,128]{1,0:T(4,128)}, u32[]{:S(2)}) copy-start(f32[4,128]{1,0:T(4,128)} %second.1) | copy-start | bytes 6148
  65.0 7.8 %copy-start = (bf16[32,256]{1,0:T(8,128)(2,1)S(1)}, bf16[32,256]{1,0:T(8,128)(2,1)}, u32[]{:S(2)}) copy-start(bf16[32,256]{1,0:T(8,128)(2,1)} %basis.3) | copy-start | bytes 49156
  72.8 11.5 %copy-start.2 = (f32[32,128]{1,0:T(8,128)S(1)}, f32[32,128]{1,0:T(8,128)}, u32[]{:S(2)}) copy-start(f32[32,128]{1,0:T(8,128)} %master.1) | copy-start | bytes 49156

commit v7 on v6

--- a/solution.py
+++ b/solution.py
@@ -67,13 +67,14 @@
         fetches.append(pltpu.make_async_copy(inputs.at[part], held.at[part], sems.at[1 + i]))
     for fetch in fetches:
         fetch.start()
-    rank = lax.broadcasted_iota(jnp.int32, (RANK, PER), 0)
-    slot = lax.broadcasted_iota(jnp.int32, (RANK, PER), 1)
+    rank = lax.broadcasted_iota(jnp.int32, (RANK, DQK), 0)
+    slot = lax.broadcasted_iota(jnp.int32, (RANK, DQK), 1) % PER
     wanted = (slot // OWN) * PER + OWN * lax.axis_index(TP) + slot % OWN
     chosen = (rank == wanted).astype(F32).astype(BF16)
     near.wait()
     mine = jnp.dot(rows[...], chosen, preferred_element_type=F32)
-    wide = jnp.concatenate([mine[8 * q : 8 * q + 8] for q in range(4)], axis=1)
+    lane = lax.broadcasted_iota(jnp.int32, (8, DQK), 1) // PER
+    wide = sum(jnp.where(lane == q, mine[8 * q : 8 * q + 8], 0.0) for q in range(4))
     out[...] = copies(wide.astype(BF16), out.shape[0])
     for fetch in fetches:
         fetch.wait()

time: 85.4 us -> 85.4 us (level)
  no operation moved by 1% of the time
where the time goes in v7:
time: 85.4 us; the launch traced here: 85 us
  blocking collectives  81.4 us (95%)
  Pallas kernels  2.82 us (3%)
    all_to_all x5, blocking collectives, exchange(): lax.all_to_all(parts, axes, 0, 0, axis_index_groups=groups, tiled=True)  65.5 us
    all_to_all x1, blocking collectives, body(): lax.all_to_all(low, ('zh', 'zl'), 0, 0, axis_index_groups=groups, tiled=T...  15.9 us
    pallas_call x7, Pallas kernels, call(): pl.pallas_call(kernel, out_shape=out, in_specs=[pl.BlockSpec(memory_space...  2.82 us

profile of v7, /device:TPU:1, one launch (start us, length us, event | category | flops | bytes accessed | tf_op | source)
XLA Modules:
  0.0 85.0 jit_solution(9869623497671102679)
XLA Ops:
  0.6 1.2 %pick.1 = (bf16[64,8,128]{2,1,0:T(8,128)(2,1)S(1)}, bf16[256,2048]{1,0:T(8,128)(2,1)S(1)}) custom-call(bf16[256,2048]{1,0:T(8,128)(2,1)} %inputs.1, bf16[32,256]{1,0:T(8,128)(2,1)} %basis.3), custom_call_target="tpu_custom_call" | custom-call | flops 200000 | bytes 1064960 | tf_op jit(solution)/shard_map/pick/pallas_call | solution.py:38
  1.9 27.9 %all_to_all.30.columns = bf16[64,8,128]{2,1,0:T(8,128)(2,1)S(1)} all-to-all(bf16[64,8,128]{2,1,0:T(8,128)(2,1)S(1)} %get-tuple-element.12), channel_id=1, replica_groups={{376,384,392,400,408,416,424,432,440,448,456,464,472,480,488,496,504,0,..., dimensions={0} | all-to-all | bytes 262144 | tf_op jit(solution)/shard_map/columns/all_to_all | solution.py:54
  29.7 0.5 project.1
  30.2 0.0 copy-start.1
  30.3 10.9 %all_to_all.31.both = bf16[8,64,256]{2,1,0:T(8,128)(2,1)S(1)} all-to-all(bf16[8,64,256]{2,1,0:T(8,128)(2,1)S(1)} %project.1), channel_id=1, replica_groups={{5,6,7,0,1,2,3,4},{13,14,15,8,9,10,11,12},{21,22,23,16,17,18,19,20},{29..., dimensions={0} | all-to-all | bytes 524288 | tf_op jit(solution)/shard_map/ranks/all_to_all | solution.py:54
  41.1 0.0 copy-done.1
  41.1 0.2 low.1
  41.3 0.0 copy-start.3
  41.3 0.0 copy-start.4
  41.4 7.6 %all_to_all.32.parts = f32[8,32,128]{2,1,0:T(8,128)S(1)} all-to-all(f32[8,32,128]{2,1,0:T(8,128)S(1)} %low.1), channel_id=1, replica_groups={{48,56,0,8,16,24,32,40},{49,57,1,9,17,25,33,41},{50,58,2,10,18,26,34,42..., dimensions={0} | all-to-all | bytes 262144 | tf_op jit(solution)/shard_map/near_sum/all_to_all | solution.py:54
  49.0 0.0 copy-done.3
  49.0 0.0 copy-done.4
  49.0 15.9 %all_to_all.33.parts = f32[8,40,128]{2,1,0:T(8,128)S(1)} all-to-all(f32[8,40,128]{2,1,0:T(8,128)S(1)} %sum_near.1), channel_id=1, replica_groups={{320,384,448,0,64,128,192,256},{288,352,416,480,32,96,160,224},{321,385..., dimensions={0} | all-to-all | bytes 327680 | tf_op jit(solution)/shard_map/far_sum/all_to_all | solution.py:190
  65.0 0.0 copy-start
  65.0 7.8 %all_to_all.34.parts = f32[8,32,128]{2,1,0:T(8,128)S(1)} all-to-all(f32[8,32,128]{2,1,0:T(8,128)S(1)} %get-tuple-element.13), channel_id=1, replica_groups={{48,56,0,8,16,24,32,40},{49,57,1,9,17,25,33,41},{50,58,2,10,18,26,34,42..., dimensions={0} | all-to-all | bytes 262144 | tf_op jit(solution)/shard_map/updates/all_to_all | solution.py:54
  72.8 0.0 copy-done
  72.8 0.0 copy-start.2
  72.8 0.2 apply.1
  73.0 11.3 %all_to_all.35.squares = f32[8,1,128]{2,1,0:T(1,128)S(1)} all-to-all(f32[8,1,128]{2,1,0:T(1,128)S(1)} %get-tuple-element.14.own), channel_id=1, replica_groups={{5,6,7,0,1,2,3,4},{13,14,15,8,9,10,11,12},{21,22,23,16,17,18,19,20},{29..., dimensions={0} | all-to-all | bytes 8192 | tf_op jit(solution)/shard_map/squares/all_to_all | solution.py:54
  84.3 0.0 copy-done.2
  84.3 0.6 scale.1
  (2 shorter events, 0.1 us)
Async XLA Ops:
  30.2 10.9 %copy-start.1 = (bf16[256,128]{1,0:T(8,128)(2,1)S(1)}, bf16[256,128]{1,0:T(8,128)(2,1)}, u32[]{:S(2)}) copy-start(bf16[256,128]{1,0:T(8,128)(2,1)} %cot.1) | copy-start | bytes 196612
  41.3 7.7 %copy-start.3 = (f32[4,128]{1,0:T(4,128)S(1)}, f32[4,128]{1,0:T(4,128)}, u32[]{:S(2)}) copy-start(f32[4,128]{1,0:T(4,128)} %first.1) | copy-start | bytes 6148
  41.3 7.6 %copy-start.4 = (f32[4,128]{1,0:T(4,128)S(1)}, f32[4,128]{1,0:T(4,128)}, u32[]{:S(2)}) copy-start(f32[4,128]{1,0:T(4,128)} %second.1) | copy-start | bytes 6148
  65.0 7.8 %copy-start = (bf16[32,256]{1,0:T(8,128)(2,1)S(1)}, bf16[32,256]{1,0:T(8,128)(2,1)}, u32[]{:S(2)}) copy-start(bf16[32,256]{1,0:T(8,128)(2,1)} %basis.3) | copy-start | bytes 49156
  72.8 11.5 %copy-start.2 = (f32[32,128]{1,0:T(8,128)S(1)}, f32[32,128]{1,0:T(8,128)}, u32[]{:S(2)}) copy-start(f32[32,128]{1,0:T(8,128)} %master.1) | copy-start | bytes 49156
